TPU v7x, 128 devices: a whole 4x4x4 slice. The times are simulated.
128 devices in a mesh: kv: 16 (over z, x), tp: 8 (over y, core).
Axes of the slice: x: 4, y: 4, z: 4, core: 2. Of those that a mesh axis runs over, the one named last changes fastest.
Arguments:
- tokens: bfloat16 [64, 2048], P(None, 'kv'), may hold values from -6 to 6
- token_gain: float32 [2048], P('kv'), may hold values from 0.1 to 1.9
- w_query: bfloat16 [2048, 1536], P('kv', 'tp'), may hold values from -0.125 to 0.125
- w_down_kv: bfloat16 [2048, 512], P('kv'), may hold values from -0.125 to 0.125
- w_rope_key: bfloat16 [2048, 64], P('kv'), may hold values from -0.125 to 0.125
- latent_gain: float32 [512], replicated, may hold values from 0.1 to 1.9
- w_key_up: bfloat16 [8, 512, 128], P('tp'), may hold values from -0.25 to 0.25
- w_value_up: bfloat16 [8, 512, 128], P('tp'), may hold values from -0.25 to 0.25
- w_out: bfloat16 [1024, 2048], P('tp', 'kv'), may hold values from -0.1875 to 0.1875
- out_gain: float32 [2048], P('kv'), may hold values from 0.1 to 1.9
- cache_latent: bfloat16 [64, 8192, 512], P('tp', 'kv'), may hold values from -6 to 6
- cache_rope: bfloat16 [64, 8192, 64], P('tp', 'kv'), may hold values from -6 to 6
- lengths: int32 [64], replicated, may hold values from 1 to 8191, as said below
Outputs:
- mixed: bfloat16 [64, 2048], P(None, 'kv')
Inputs may be any that keep to these rules, and one draw needn't show every extreme that they name: `lengths`: each of the 64 sequences has 1 to 8191 cached positions; some sequence has exactly 8191 and some exactly 1.
All inputs are finite; a program needn't handle non-finite values.
Results may differ from a plain program's by a relative error of at most 0.015.
Values may be sent and summed in bfloat16 or wider, within the bound.
A program may use at most 64 MiB of HBM per device.

v0:
```python
import functools

import jax
import jax.numpy as jnp
from jax import lax
from jax.experimental import pallas as pl
from jax.experimental.pallas import tpu as pltpu
from jax.sharding import PartitionSpec as P

EPSILON = 1e-06
NEGATIVE = -1e30
LANES = 128
MESH = pl.DeviceIdType.MESH
F32 = jnp.float32
BF16 = jnp.bfloat16


def rounded(values):
    return values.astype(BF16).astype(F32)


def rotated(values, cosine, signed_sine, half):
    lane = lax.broadcasted_iota(jnp.int32, values.shape, 1)
    swapped = jnp.where(
        lane < half, pltpu.roll(values, LANES - half, 1), pltpu.roll(values, half, 1)
    )
    return values * cosine + swapped * signed_sine


def dot_t(a, b):
    return lax.dot_general(a, b, (((1,), (1,)), ((), ())), preferred_element_type=F32)


def kernel(
    kv,
    tp,
    lengths,
    tok_h,
    tgain_h,
    wq_h,
    wd_h,
    wr_h,
    cos_h,
    sin_h,
    wku_h,
    cl_h,
    cr_h,
    lgain_h,
    wvu_h,
    wo_h,
    ogain_h,
    out,
    tok,
    tgain,
    wq,
    wd,
    wr,
    cos,
    sin,
    wku,
    cl,
    cr,
    lgain,
    wvu,
    wo,
    ogain,
    scaled_s,
    q_send,
    q_recv,
    lat_send,
    lat_recv,
    row_send,
    row_recv,
    ql_send,
    ql_recv,
    q32,
    stage,
    part_send,
    part_recv,
    hl_send,
    hl_recv,
    mix_send,
    mix_recv,
    sq_send,
    sq_recv,
    in_sem,
    q_ss,
    q_rs,
    lat_ss,
    lat_rs,
    row_ss,
    row_rs,
    ql_ss,
    ql_rs,
    part_ss,
    part_rs,
    hl_ss,
    hl_rs,
    mix_ss,
    mix_rs,
    sq_ss,
    sq_rs,
):
    k = lax.axis_index("kv")
    t = lax.axis_index("tp")
    batch, width = tok.shape
    lh, latent, nope_w = wku.shape
    rope_w = wr.shape[0]
    head_w = nope_w + rope_w
    half = rope_w // 2
    factor = head_w ** (-0.5)
    seqs, pos = cl.shape[0], cl.shape[1]
    heads = lh * tp
    full = latent + LANES
    per_row = kv // tp
    dup = per_row // lh
    lat_dup = kv // seqs
    rows = heads * seqs // kv
    parts = seqs // rows
    model_w = width * kv
    chunk = q_send.shape[2]

    loads = [
        pltpu.make_async_copy(a, b, in_sem.at[i])
        for i, (a, b) in enumerate(
            [
                (tok_h, tok),
                (tgain_h, tgain),
                (wq_h, wq),
                (wd_h, wd),
                (wr_h, wr),
                (cos_h, cos),
                (sin_h, sin),
                (wku_h, wku),
                (lgain_h, lgain),
                (cl_h, cl),
                (cr_h, cr),
                (wvu_h, wvu),
                (wo_h, wo),
                (ogain_h, ogain),
            ]
        )
    ]
    for load in loads:
        load.start()

    barrier = pltpu.get_barrier_semaphore()
    me = k * tp + t

    def greet(i, carry):
        @pl.when(i != me)
        def _():
            pl.semaphore_signal(
                barrier, inc=1, device_id=(i // tp, i % tp), device_id_type=MESH
            )

        return carry

    lax.fori_loop(0, kv * tp, greet, 0)

    def remote(src, dst, send, recv, kk, tt):
        return pltpu.make_async_remote_copy(
            src_ref=src,
            dst_ref=dst,
            send_sem=send,
            recv_sem=recv,
            device_id=(kk, tt),
            device_id_type=MESH,
        )

    def push(src, dst, send, recv, kk, tt):
        same = jnp.logical_and(kk == k, tt == t)

        @pl.when(jnp.logical_not(same))
        def _():
            remote(src, dst, send, recv, kk, tt).start()

        @pl.when(same)
        def _():
            pltpu.make_async_copy(src, dst, recv).start()

    def pushed(src, dst, send, recv, kk, tt):
        same = jnp.logical_and(kk == k, tt == t)

        @pl.when(jnp.logical_not(same))
        def _():
            remote(src, dst, send, recv, kk, tt).wait_send()

    def each(count, body):
        def step(i, carry):
            body(i)
            return carry

        lax.fori_loop(0, count, step, 0)

    def arrive(buffer, sems, count):
        each(
            count,
            lambda i: pltpu.make_async_copy(buffer.at[i], buffer.at[i], sems.at[i]).wait(),
        )

    for i in range(3):
        loads[i].wait()
    scaled = (tok[...].astype(F32) * tgain[...]).astype(BF16)
    query = jnp.dot(scaled, wq[...], preferred_element_type=F32)
    if query.shape[1] % LANES:
        pad = LANES - query.shape[1] % LANES
        query = jnp.concatenate([query, jnp.zeros((batch, pad), F32)], axis=1)
    for dest in range(kv):
        group, head = dest // per_row, (dest % per_row) % lh
        first = head * head_w // LANES * LANES
        q_send[dest] = query[group * seqs : (group + 1) * seqs, first : first + chunk]
    wide = scaled.astype(F32)
    for group in range(tp):
        scaled_s[group] = wide[group * seqs : (group + 1) * seqs]
    own = scaled_s[t].astype(BF16)
    loads[3].wait()
    loads[4].wait()
    lat = jnp.dot(own, wd[...], preferred_element_type=F32)
    rope = dot_t(own, wr[...])
    for i in range(seqs):
        lat_send[i, :, :latent] = lat[i : i + 1]
        lat_send[i, :, latent:] = jnp.zeros((1, LANES), F32)
        lat_send[i, :, latent : latent + rope_w] = rope[i : i + 1]

    pl.semaphore_wait(barrier, kv * tp - 1)

    q_args = lambda i: (q_send.at[i], q_recv.at[k], q_ss.at[i], q_rs.at[k], i, t)
    lat_args = lambda i: (
        lat_send.at[i // lat_dup],
        lat_recv.at[k],
        lat_ss.at[i],
        lat_rs.at[k],
        i,
        t,
    )
    each(kv, lambda i: push(*q_args(i)))
    each(kv, lambda i: push(*lat_args(i)))

    group = k // per_row
    head = (k % per_row) % lh
    copy_at = (k % per_row) // lh
    for i in range(5, 8):
        loads[i].wait()
    arrive(q_recv, q_rs, kv)
    query = q_recv[0]
    for i in range(1, kv):
        query = query + q_recv[i]
    query = rounded(query)
    if lh > 1:
        shift = head * head_w % LANES
        query = jnp.where(shift == 0, query, pltpu.roll(query, chunk - head_w % LANES, 1))
    spun = rotated(query[:, nope_w : nope_w + LANES], cos[group], sin[group], half)
    ql_send[:, :latent] = dot_t(query[:, :nope_w].astype(BF16), wku[head]).astype(BF16)
    ql_send[:, latent:] = spun.astype(BF16)
    ql_args = lambda i: (
        ql_send,
        ql_recv.at[t * lh + head],
        ql_ss.at[i],
        ql_rs.at[t * lh + head],
        copy_at + dup * i,
        group,
    )
    each(kv // dup, lambda i: push(*ql_args(i)))

    loads[8].wait()
    arrive(lat_recv, lat_rs, kv)
    fresh = lat_recv[0]
    for i in range(1, kv):
        fresh = fresh + lat_recv[i]
    fresh_lat = fresh[:, :latent]
    scale = lax.rsqrt(jnp.mean(fresh_lat * fresh_lat, axis=1, keepdims=True) + EPSILON)
    seq = k // lat_dup
    pick = lax.broadcasted_iota(jnp.int32, (seqs, LANES), 0) == seq
    own_cos = jnp.sum(jnp.where(pick, cos[t], 0.0), axis=0, keepdims=True)
    own_sin = jnp.sum(jnp.where(pick, sin[t], 0.0), axis=0, keepdims=True)
    row_send[:, :latent] = rounded(fresh_lat * scale * lgain[...])
    row_send[:, latent:] = rounded(rotated(fresh[:, latent:], own_cos, own_sin, half))
    row_args = lambda i: (
        row_send,
        row_recv.at[seq],
        row_ss.at[i],
        row_rs.at[seq],
        k % lat_dup + lat_dup * i,
        t,
    )
    each(kv // lat_dup, lambda i: push(*row_args(i)))

    loads[9].wait()
    loads[10].wait()
    arrive(ql_recv, ql_rs, heads)
    for i in range(heads):
        wide = ql_recv[i].astype(F32)
        for c in range(full // LANES):
            q32[c, i * seqs : (i + 1) * seqs, :] = wide[:, c * LANES : (c + 1) * LANES]
    place = k * pos + lax.broadcasted_iota(jnp.int32, (heads, pos), 1)
    lane = lax.broadcasted_iota(jnp.int32, (heads, LANES), 1)
    all_scores = []
    for b in range(seqs):
        q_b = jnp.concatenate(
            [q32[c, pl.ds(b, heads, stride=seqs), :] for c in range(full // LANES)], axis=1
        ).astype(BF16)
        all_scores.append(
            (
                dot_t(q_b[:, :latent], cl[b])
                + jnp.dot(
                    q_b[:, latent : latent + rope_w], cr[b], preferred_element_type=F32
                )
            )
            * factor
        )
    for b in range(seqs):
        visible = place < lengths[t * seqs + b]
        scores = jnp.where(visible, all_scores[b], NEGATIVE)
        top = jnp.max(scores, axis=1, keepdims=True)
        weights = jnp.where(visible, jnp.exp(scores - top), 0.0)
        total = jnp.sum(weights, axis=1, keepdims=True)
        acc = jnp.dot(weights.astype(BF16), cl[b], preferred_element_type=F32)
        stats = jnp.zeros((heads, LANES), F32)
        for at, value in ((0, top), (3, total)):
            for i in range(3):
                piece = rounded(value)
                stats = jnp.where(lane == at + i, piece, stats)
                value = value - piece
        for c in range(latent // LANES):
            stage[c, pl.ds(b, heads, stride=seqs), :] = acc[:, c * LANES : (c + 1) * LANES]
        stage[latent // LANES, pl.ds(b, heads, stride=seqs), :] = stats
    for dest in range(kv):
        for c in range(full // LANES):
            part_send[dest, :, c * LANES : (c + 1) * LANES] = stage[
                c, dest * rows : (dest + 1) * rows, :
            ].astype(BF16)
    part_args = lambda i: (part_send.at[i], part_recv.at[k], part_ss.at[i], part_rs.at[k], i, t)
    each(kv, lambda i: push(*part_args(i)))

    head_at = k // parts
    part_at = k % parts
    arrive(row_recv, row_rs, seqs)
    new_key = jnp.concatenate([row_recv[i] for i in range(seqs)], axis=0)
    own_query = ql_recv[head_at].astype(F32)

    def part_of(values):
        result = values[:rows]
        for i in range(1, parts):
            result = jnp.where(part_at == i, values[i * rows : (i + 1) * rows], result)
        return result

    new_key = part_of(new_key)
    own_query = part_of(own_query)
    new_score = jnp.sum(own_query * new_key, axis=1, keepdims=True) * factor
    arrive(part_recv, part_rs, kv)
    tops, sums, accs = [], [], []
    best = new_score
    for i in range(kv):
        stats = part_recv[i, :, latent:].astype(F32)
        top = stats[:, 0:1] + stats[:, 1:2] + stats[:, 2:3]
        tops.append(top)
        sums.append(stats[:, 3:4] + stats[:, 4:5] + stats[:, 5:6])
        best = jnp.maximum(best, top)
    new_weight = jnp.exp(new_score - best)
    weighted = rounded(new_weight) * new_key[:, :latent]
    weight_sum = new_weight
    for i in range(kv):
        share = jnp.exp(tops[i] - best)
        weight_sum = weight_sum + share * sums[i]
        weighted = weighted + share * part_recv[i, :, :latent].astype(F32)
    hl_send[...] = (weighted / weight_sum).astype(BF16)
    slot = (head_at % lh) * (tp * parts) + t * parts + part_at
    hl_args = lambda i: (
        hl_send,
        hl_recv.at[slot],
        hl_ss.at[i],
        hl_rs.at[slot],
        i,
        head_at // lh,
    )
    each(kv, lambda i: push(*hl_args(i)))

    for i in range(11, 14):
        loads[i].wait()
    arrive(hl_recv, hl_rs, lh * tp * parts)
    outs = []
    for i in range(lh):
        base = i * tp * parts
        block = jnp.concatenate(
            [hl_recv[base + j].astype(F32) for j in range(tp * parts)], axis=0
        ).astype(BF16)
        outs.append(jnp.dot(block, wvu[i], preferred_element_type=F32).astype(BF16))
    head_out = outs[0] if lh == 1 else jnp.concatenate(outs, axis=1)
    mix_send[...] = jnp.dot(head_out, wo[...], preferred_element_type=F32).astype(BF16)
    mix_args = lambda i: (mix_send, mix_recv.at[t], mix_ss.at[i], mix_rs.at[t], k, i)
    each(tp, lambda i: push(*mix_args(i)))
    arrive(mix_recv, mix_rs, tp)
    mixed = mix_recv[0].astype(F32)
    for i in range(1, tp):
        mixed = mixed + mix_recv[i].astype(F32)

    squares = jnp.sum(mixed * mixed, axis=1, keepdims=True)
    diagonal = lax.broadcasted_iota(jnp.int32, (batch, LANES), 0) == lax.broadcasted_iota(
        jnp.int32, (batch, LANES), 1
    )
    sq_send[...] = jnp.broadcast_to(
        jnp.sum(jnp.where(diagonal, squares, 0.0), axis=0, keepdims=True), sq_send.shape
    )
    sq_args = lambda i: (sq_send, sq_recv.at[k], sq_ss.at[i], sq_rs.at[k], i, t)
    each(kv, lambda i: push(*sq_args(i)))
    arrive(sq_recv, sq_rs, kv)
    line = sq_recv[0]
    for i in range(1, kv):
        line = line + sq_recv[i]
    squares = jnp.sum(jnp.where(diagonal, line[0:1], 0.0), axis=1, keepdims=True)
    out[...] = (mixed * lax.rsqrt(squares / model_w + EPSILON) * ogain[...]).astype(out.dtype)

    each(kv, lambda i: pushed(*q_args(i)))
    each(kv, lambda i: pushed(*lat_args(i)))
    each(kv // dup, lambda i: pushed(*ql_args(i)))
    each(kv // lat_dup, lambda i: pushed(*row_args(i)))
    each(kv, lambda i: pushed(*part_args(i)))
    each(kv, lambda i: pushed(*hl_args(i)))
    each(tp, lambda i: pushed(*mix_args(i)))
    each(kv, lambda i: pushed(*sq_args(i)))


def on_device(
    kv,
    tp,
    tokens,
    token_gain,
    w_query,
    w_down_kv,
    w_rope_key,
    latent_gain,
    w_key_up,
    w_value_up,
    w_out,
    out_gain,
    cache_latent,
    cache_rope,
    lengths,
):
    batch = tokens.shape[0]
    lh, latent, nope_w = w_key_up.shape
    rope_w = w_rope_key.shape[1]
    seqs = cache_latent.shape[0]
    heads = lh * tp
    full = latent + LANES
    rows = heads * seqs // kv
    per_row = kv // tp
    parts = seqs // rows
    assert kv % tp == 0 and per_row % lh == 0 and kv % seqs == 0
    assert seqs % rows == 0 and batch == seqs * tp and batch <= LANES
    dup = per_row // lh
    lat_dup = kv // seqs
    chunk = -(-(nope_w + rope_w) // LANES) * LANES

    inverse_freq = 1.0 / 10000.0 ** (jnp.arange(0, rope_w, 2, dtype=F32) / rope_w)
    angles = lengths.astype(F32)[:, None] * inverse_freq[None, :]
    cosine, sine = jnp.cos(angles), jnp.sin(angles)
    blank = jnp.zeros((batch, LANES - rope_w), F32)
    cos = jnp.concatenate([cosine, cosine, blank], axis=1).reshape(tp, seqs, LANES)
    sin = jnp.concatenate([-sine, sine, blank], axis=1).reshape(tp, seqs, LANES)

    arrays = [
        tokens,
        token_gain[None, :],
        w_query,
        w_down_kv,
        w_rope_key.T,
        cos,
        sin,
        w_key_up,
        cache_latent,
        jnp.swapaxes(cache_rope, 1, 2),
        latent_gain[None, :],
        w_value_up,
        w_out,
        out_gain[None, :],
    ]
    columns = w_out.shape[1]
    dma = lambda n: pltpu.SemaphoreType.DMA((n,))
    slots = lh * tp * parts
    return pl.pallas_call(
        functools.partial(kernel, kv, tp),
        out_shape=jax.ShapeDtypeStruct((batch, columns), BF16),
        in_specs=[pl.BlockSpec(memory_space=pltpu.SMEM)]
        + [pl.BlockSpec(memory_space=pl.ANY)] * len(arrays),
        out_specs=pl.BlockSpec(memory_space=pltpu.VMEM),
        scratch_shapes=[pltpu.VMEM(a.shape, a.dtype) for a in arrays]
        + [
            pltpu.VMEM((tp, seqs, tokens.shape[1]), F32),
            pltpu.VMEM((kv, seqs, chunk), F32),
            pltpu.VMEM((kv, seqs, chunk), F32),
            pltpu.VMEM((seqs, 1, full), F32),
            pltpu.VMEM((kv, 1, full), F32),
            pltpu.VMEM((1, full), F32),
            pltpu.VMEM((seqs, 1, full), F32),
            pltpu.VMEM((seqs, full), BF16),
            pltpu.VMEM((heads, seqs, full), BF16),
            pltpu.VMEM((full // LANES, heads * seqs, LANES), F32),
            pltpu.VMEM((full // LANES, heads * seqs, LANES), F32),
            pltpu.VMEM((kv, rows, full), BF16),
            pltpu.VMEM((kv, rows, full), BF16),
            pltpu.VMEM((rows, latent), BF16),
            pltpu.VMEM((slots, rows, latent), BF16),
            pltpu.VMEM((batch, columns), BF16),
            pltpu.VMEM((tp, batch, columns), BF16),
            pltpu.VMEM((8, LANES), F32),
            pltpu.VMEM((kv, 8, LANES), F32),
            dma(len(arrays)),
            dma(kv),
            dma(kv),
            dma(kv),
            dma(kv),
            dma(kv // lat_dup),
            dma(seqs),
            dma(kv // dup),
            dma(heads),
            dma(kv),
            dma(kv),
            dma(kv),
            dma(slots),
            dma(tp),
            dma(tp),
            dma(kv),
            dma(kv),
        ],
        compiler_params=pltpu.CompilerParams(
            collective_id=0, has_side_effects=True, vmem_limit_bytes=56 * 1024 * 1024
        ),
        name="decode",
    )(lengths, *arrays)


def solution(mesh):
    placed = (
        P(None, "kv"),
        P("kv"),
        P("kv", "tp"),
        P("kv", None),
        P("kv", None),
        P(),
        P("tp", None, None),
        P("tp", None, None),
        P("tp", "kv"),
        P("kv"),
        P("tp", "kv", None),
        P("tp", "kv", None),
        P(),
    )
    return jax.shard_map(
        functools.partial(on_device, mesh.shape["kv"], mesh.shape["tp"]),
        mesh=mesh,
        in_specs=placed,
        out_specs=P(None, "kv"),
        check_vma=False,
    )
```

profile of v0, /device:TPU:1, one launch (start us, length us, event | category | flops | bytes accessed | tf_op | source)
XLA Modules:
  0.0 50.2 jit_solution(7085652343862656953)
XLA Ops:
  0.0 0.7 %convert_element_type.3 = f32[64]{0:T(128)S(1)} convert(s32[64]{0:T(128)} %lengths.1) | non-fusion elementwise | flops 64 | bytes 512 | tf_op jit(solution)/shard_map/convert_element_type | solution.py:457
  0.7 0.1 mul.22
  0.8 0.2 fusion
  1.0 0.1 pad.5.clone
  1.0 0.7 %maximum_maximum_fusion.1 = (f32[8,8,128]{2,1,0:T(8,128)}, f32[8,8,128]{2,1,0:T(8,128)}) fusion(f32[8,8,32]{2,1,0:T(8,128)S(1)} %get-tuple-element.6, f32[8,8,32]{2,1,0:T(8,128)S(1)} %get-tuple-element.5, f32[128]{0:T(128)S(1)} %pad.5.clone, f32[8,8,32]{2,1,0:T(8,128)S(1)} %get-tuple-element.7), kind=kLoop, calls=%fused_computation.3 | loop fusion | flops 32768 | bytes 90624 | tf_op jit(solution)/shard_map/concatenate | solution.py:461
  1.8 1.5 %copy.14.wq_h = bf16[128,192]{1,0:T(8,128)(2,1)} copy(bf16[128,192]{0,1:T(8,128)(2,1)} %param.15) | data formatting | bytes 98304 | tf_op args[2]
  3.3 45.6 %decode.1 = bf16[64,128]{1,0:T(8,128)(2,1)} custom-call(s32[64]{0:T(128)} %lengths.1, bf16[64,128]{1,0:T(8,128)(2,1)} %tok_h.1, f32[1,128]{1,0:T(1,128)} %bitcast.8, bf16[128,192]{1,0:T(8,128)(2,1)} %copy.14.wq_h, bf16[128,512]{1,0:T(8,128)(2,1)} %wd_h.1, bf16[64,128]{1,0:T(8,128)(2,1)} %bitcast.6, f32[8,8,128]{2,1,0:T(8,128)} %get-tuple-element.9.cos_h, ...), custom_call_target="tpu_custom_call" | custom-call | tf_op jit(solution)/shard_map/decode/pallas_call | solution.py:482
  48.9 1.3 %copy.16 = bf16[64,128]{1,0:T(8,128)(2,1)} copy(bf16[64,128]{1,0:T(8,128)(2,1)} %decode.1) | data formatting | bytes 32768
  (2 shorter events, 0.0 us)
where the time goes:
time: 50.5 us; the launch traced here: 50.2 us
  Pallas kernels  45.6 us (90%)
  local copies, waits for them, and re-layouts  2.99 us (6%)
  other arithmetic  1.57 us (3%)
    pallas_call x1, Pallas kernels, on_device(): pl.pallas_call(functools.partial(kernel, kv, tp), out_shape=jax.ShapeDtyp...  45.6 us
    unnamed x2, local copies, waits for them, and re-layouts  2.84 us

commit v1 on v0

v1 whole, which is shorter than its diff:
```python
import functools

import jax
import jax.numpy as jnp
import numpy as np
from jax import lax
from jax.experimental import pallas as pl
from jax.experimental.pallas import tpu as pltpu
from jax.sharding import PartitionSpec as P

EPSILON = 1e-06
NEGATIVE = -1e30
LANES = 128
MESH = pl.DeviceIdType.MESH
F32 = jnp.float32
BF16 = jnp.bfloat16
SIDE = 4
KV = 16
TP = 8
SEQS = 8
HEADS = 8
LATENT = 512
NOPE = 128
ROPE = 64
POS = 512
FULL = LATENT + LANES
ROWS = 4
FACTOR = (NOPE + ROPE) ** (-0.5)
MODEL = 2048


def ring_distance(d):
    return min(d % SIDE, -d % SIDE)


PLANE = sorted(
    [(a, b) for a in range(SIDE) for b in range(SIDE) if (a, b) != (0, 0)],
    key=lambda d: -(ring_distance(d[0]) + ring_distance(d[1])),
)
LINE = sorted(
    [(a, b) for a in range(SIDE) for b in range(2) if (a, b) != (0, 0)],
    key=lambda d: -(2 * ring_distance(d[0]) + d[1]),
)
EVERYWHERE = sorted(
    [
        (a, b, c, d)
        for a in range(SIDE)
        for b in range(SIDE)
        for c in range(SIDE)
        for d in range(2)
        if (a, b, c, d) != (0, 0, 0, 0)
    ],
    key=lambda d: -(2 * sum(ring_distance(i) for i in d[:3]) + d[3]),
)


def rounded(values):
    return values.astype(BF16).astype(F32)


def dot_t(a, b):
    return lax.dot_general(a, b, (((1,), (1,)), ((), ())), preferred_element_type=F32)


def dot(a, b):
    return jnp.dot(a, b, preferred_element_type=F32)


def rotated(values, cosine, signed_sine):
    half = ROPE // 2
    lane = lax.broadcasted_iota(jnp.int32, values.shape, 1)
    swapped = jnp.where(
        lane % ROPE < half,
        pltpu.roll(values, LANES - half, 1),
        pltpu.roll(values, half, 1),
    )
    return values * cosine + swapped * signed_sine


def kernel(
    lengths,
    freq_h,
    tok_h,
    tgain_h,
    wq_h,
    wd_h,
    wr_h,
    wku_h,
    cl_h,
    cr_h,
    lgain_h,
    wvu_h,
    wo_h,
    ogain_h,
    out,
    freq,
    tok,
    tgain,
    wq,
    wd,
    wr,
    wku,
    cl,
    cr,
    lgain,
    wvu,
    ogain,
    wo_all,
    wkut,
    clt,
    scaled_s,
    q_send,
    q_recv,
    lat_send,
    lat_recv,
    row_send,
    row_recv,
    ql_send,
    ql_recv,
    qm,
    qr,
    wm,
    part_send,
    part_recv,
    wv_recv,
    ho_send,
    ho_recv,
    sq_send,
    sq_recv,
    in_sem,
    ss,
    q_rs,
    lat_rs,
    row_rs,
    ql_rs,
    part_rs,
    wv_rs,
    wo_rs,
    ho_rs,
    sq_rs,
    ql_ss,
    row_ss,
    lat_ss,
):
    k = lax.axis_index("kv")
    t = lax.axis_index("tp")
    z, x = k // SIDE, k % SIDE
    y, core = t // 2, t % 2

    def load(i, a, b):
        copy = pltpu.make_async_copy(a, b, in_sem.at[i])
        copy.start()
        return copy

    half_w = NOPE + ROPE
    first = [
        load(0, tok_h, tok),
        load(1, tgain_h, tgain),
        load(2, wq_h, wq.at[pl.ds(0, half_w)]),
        load(3, wq_h.at[pl.ds(NOPE, ROPE)], wq.at[pl.ds(half_w, ROPE)]),
    ]
    load_lat = [
        load(4, wd_h, wd),
        load(5, wr_h, wr.at[pl.ds(0, ROPE)]),
        load(6, freq_h, freq),
    ]
    load_up = [load(7, wku_h, wku)]
    load_cl = [load(8, cl_h, cl)]
    load_cr = [load(9, cr_h, cr)]
    load_wvu = load(10, wvu_h, wvu)
    load_wo = load(11, wo_h, wo_all.at[t])
    load_gain = [load(12, lgain_h, lgain), load(13, ogain_h, ogain)]

    def at_plane(d):
        return ((z + d[0]) % SIDE) * SIDE + (x + d[1]) % SIDE

    def at_line(d):
        return ((y + d[0]) % SIDE) * 2 + (core + d[1]) % 2

    barrier = pltpu.get_barrier_semaphore()
    for d in PLANE:
        pl.semaphore_signal(barrier, inc=1, device_id=(at_plane(d), t), device_id_type=MESH)
    for d in LINE:
        pl.semaphore_signal(barrier, inc=1, device_id=(k, at_line(d)), device_id_type=MESH)

    def remote(src, dst, send, recv, kk, tt):
        return pltpu.make_async_remote_copy(
            src_ref=src,
            dst_ref=dst,
            send_sem=send,
            recv_sem=recv,
            device_id=(kk, tt),
            device_id_type=MESH,
        )

    def push(src, dst, send, recv, kk, tt):
        same = jnp.logical_and(kk == k, tt == t)

        @pl.when(jnp.logical_not(same))
        def _():
            remote(src, dst, send, recv, kk, tt).start()

        @pl.when(same)
        def _():
            pltpu.make_async_copy(src, dst, recv).start()

    def pushed(src, dst, send, recv, kk, tt):
        same = jnp.logical_and(kk == k, tt == t)

        @pl.when(jnp.logical_not(same))
        def _():
            remote(src, dst, send, recv, kk, tt).wait_send()

    def wait_bytes(ref, sem):
        pltpu.make_async_copy(ref, ref, sem).wait()

    with jax.named_scope("q_partial"):
        for c in first:
            c.wait()
        scaled = (tok[...].astype(F32) * tgain[...]).astype(BF16)
        query = dot_t(scaled, wq[...]).astype(BF16)
        for p in range(4):
            q_send[p] = query[16 * p : 16 * p + 16]
        mine = (x + 2 * z) % 4
        q_recv[k] = q_send[mine]
        wide = scaled.astype(F32)
        for group in range(TP):
            scaled_s[group] = wide[group * SEQS : (group + 1) * SEQS]

    with jax.named_scope("barrier"):
        pl.semaphore_wait(barrier, len(PLANE) + len(LINE))

    with jax.named_scope("send_q"):
        for d in PLANE:
            kk = at_plane(d)
            server = ((x + d[1]) + 2 * (z + d[0])) % 4
            remote(q_send.at[server], q_recv.at[k], ss.at[0], q_rs, kk, t).start()

    wv_to = ((y - z) % SIDE) * 2 + (core - x // 2) % 2
    local_wv = jnp.logical_and(z == 0, x // 2 == 0)
    with jax.named_scope("send_wv"):
        load_wvu.wait()

        @pl.when(jnp.logical_not(local_wv))
        def _():
            remote(wvu, wv_recv, ss.at[1], wv_rs, k, wv_to).start()

        @pl.when(local_wv)
        def _():
            wv_recv[...] = wvu[...]

    with jax.named_scope("lat_partial"):
        for c in load_lat:
            c.wait()
        own = scaled_s[t].astype(BF16)
        lat = dot(own, wd[...])
        wr[ROPE:, :] = jnp.zeros((LANES - ROPE, LANES), BF16)
        rope = dot_t(own, wr[...])
        for i in range(SEQS):
            lat_send[i, :, :LATENT] = lat[i : i + 1]
            lat_send[i, :, LATENT:] = rope[i : i + 1]
        lat_args = lambda i: (
            lat_send.at[i // 2],
            lat_recv.at[k],
            lat_ss.at[i],
            lat_rs.at[k],
            i,
            t,
        )

        def lat_step(i, carry):
            push(*lat_args(i))
            return carry

        lax.fori_loop(0, KV, lat_step, 0)

    with jax.named_scope("tables"):
        lane = lax.broadcasted_iota(jnp.int32, (1, LANES), 1)
        sign = jnp.where(lane % ROPE < ROPE // 2, -1.0, 1.0)
        row16 = lax.broadcasted_iota(jnp.int32, (16, LANES), 0)
        len16 = jnp.zeros((16, LANES), F32)
        for i in range(16):
            len16 = jnp.where(row16 == i, lengths[mine * 16 + i].astype(F32), len16)
        angle = len16 * freq[...]
        cos16 = jnp.cos(angle)
        sin16 = jnp.sin(angle) * sign
        seq = k // 2
        angle1 = lengths[t * SEQS + seq].astype(F32) * freq[...]
        cos1 = jnp.cos(angle1)
        sin1 = jnp.sin(angle1) * sign
        row8 = lax.broadcasted_iota(jnp.int32, (SEQS, POS), 0)
        len8 = jnp.zeros((SEQS, POS), jnp.int32)
        for b in range(SEQS):
            len8 = jnp.where(row8 == b, lengths[t * SEQS + b], len8)
        place = k * POS + lax.broadcasted_iota(jnp.int32, (SEQS, POS), 1)
        left8 = len8 - place
        load_up[0].wait()
        wkut[...] = wku[0].T

    with jax.named_scope("transpose"):
        load_cl[0].wait()
        for b in range(SEQS):
            clt[b * LATENT : (b + 1) * LATENT, :] = cl[b * POS : (b + 1) * POS, :].T

    with jax.named_scope("wait_q"):
        wait_bytes(q_recv.at[pl.ds(0, KV - 1)], q_rs)

    with jax.named_scope("key_up"):
        query = q_recv[0].astype(F32)
        for i in range(1, KV):
            query = query + q_recv[i].astype(F32)
        query = rounded(query)
        spun = rotated(query[:, NOPE:], cos16, sin16)
        up = dot(query[:, :NOPE].astype(BF16), wkut[...])
        for g in range(2):
            ql_send[g, :, :LATENT] = up[g * SEQS : (g + 1) * SEQS].astype(BF16)
            ql_send[g, :, LATENT:] = spun[g * SEQS : (g + 1) * SEQS].astype(BF16)

    def ql_all(act):
        for j, d in enumerate(((0, 1), (0, -1), (-1, 0), (0, 0))):
            for g in range(2):
                act(
                    ql_send.at[g],
                    ql_recv.at[t],
                    ql_ss.at[2 * j + g],
                    ql_rs.at[t],
                    at_plane(d),
                    2 * mine + g,
                )

    with jax.named_scope("send_ql"):
        ql_all(push)

    with jax.named_scope("send_wo"):
        load_wo.wait()
        for d in LINE:
            remote(wo_all.at[t], wo_all.at[t], ss.at[2], wo_rs, k, at_line(d)).start()

    with jax.named_scope("new_row"):
        load_gain[0].wait()
        for i in range(KV):
            wait_bytes(lat_recv.at[i], lat_rs.at[i])
        fresh = lat_recv[0]
        for i in range(1, KV):
            fresh = fresh + lat_recv[i]
        fresh_lat = fresh[:, :LATENT]
        scale = lax.rsqrt(jnp.mean(fresh_lat * fresh_lat, axis=1, keepdims=True) + EPSILON)
        row_send[:, :LATENT] = rounded(fresh_lat * scale * lgain[...])
        row_send[:, LATENT:] = rounded(rotated(fresh[:, LATENT:], cos1, sin1))
        row_args = lambda i: (
            row_send,
            row_recv.at[seq % ROWS],
            row_ss.at[i],
            row_rs.at[seq % ROWS],
            2 * (4 * (k % 2) + i) + seq // ROWS,
            t,
        )
        for i in range(4):
            push(*row_args(i))

    with jax.named_scope("masks"):
        load_cr[0].wait()
        rowp = lax.broadcasted_iota(jnp.int32, (64, LANES), 0) % SEQS
        lanep = lax.broadcasted_iota(jnp.int32, (64, LANES), 1) // ROPE
        keep = [(rowp == b).astype(F32).astype(BF16) for b in range(SEQS)]
        keep_rope = [(rowp == lanep + 2 * c).astype(F32).astype(BF16) for c in range(4)]
        left = jnp.concatenate([left8] * HEADS, axis=0)
        visible = left > 0

    with jax.named_scope("wait_ql"):
        for i in range(HEADS):
            wait_bytes(ql_recv.at[i], ql_rs.at[i])

    with jax.named_scope("scores"):
        q = jnp.concatenate([ql_recv[i].astype(F32) for i in range(HEADS)], axis=0).astype(BF16)
        for c in range(LATENT // LANES):
            piece = q[:, c * LANES : (c + 1) * LANES]
            for b in range(SEQS):
                qm[:, b * LATENT + c * LANES : b * LATENT + (c + 1) * LANES] = piece * keep[b]
        piece = q[:, LATENT:]
        for c in range(4):
            qr[:, c * LANES : (c + 1) * LANES] = piece * keep_rope[c]
        scores = (dot(qm[...], clt[...]) + dot(qr[...], cr[...])) * FACTOR
    with jax.named_scope("softmax"):
        scores = jnp.where(visible, scores, NEGATIVE)
        top = jnp.max(scores, axis=1, keepdims=True)
        weights = jnp.where(visible, jnp.exp(scores - top), 0.0)
        total = jnp.sum(weights, axis=1, keepdims=True)
        wb = weights.astype(BF16)
        for c in range(POS // LANES):
            piece = wb[:, c * LANES : (c + 1) * LANES]
            for b in range(SEQS):
                wm[:, b * POS + c * LANES : b * POS + (c + 1) * LANES] = piece * keep[b]
        lane64 = lax.broadcasted_iota(jnp.int32, (64, LANES), 1)
        stats = jnp.zeros((64, LANES), F32)
        for at, value in ((0, top), (3, total)):
            for i in range(3):
                bit = rounded(value)
                stats = jnp.where(lane64 == at + i, bit, stats)
                value = value - bit
    with jax.named_scope("attend"):
        acc = dot(wm[...], cl[...])
        for i in range(KV):
            part_send[i, :, :LATENT] = acc[i * ROWS : (i + 1) * ROWS].astype(BF16)
            part_send[i, :, LATENT:] = stats[i * ROWS : (i + 1) * ROWS].astype(BF16)

    def head_of(zz, xx):
        return ((y + zz) % SIDE) * 2 + (core + (xx % SIDE) // 2) % 2

    head = head_of(z, x)
    part = x % 2
    with jax.named_scope("send_part"):
        for d in PLANE:
            index = head_of(z + d[0], x + d[1]) * 2 + (x + d[1]) % 2
            remote(
                part_send.at[index], part_recv.at[k], ss.at[3], part_rs, at_plane(d), t
            ).start()
        part_recv[k] = part_send[head * 2 + part]

    with jax.named_scope("new_score"):
        for i in range(ROWS):
            wait_bytes(row_recv.at[i], row_rs.at[i])
        new_key = jnp.concatenate([row_recv[i] for i in range(ROWS)], axis=0)
        own_query = ql_recv[head].astype(F32)
        own_query = jnp.where(part == 0, own_query[:ROWS], own_query[ROWS:])
        new_score = jnp.sum(own_query * new_key, axis=1, keepdims=True) * FACTOR

        @pl.when(jnp.logical_not(local_wv))
        def _():
            wait_bytes(wv_recv, wv_rs)

    with jax.named_scope("wait_part"):
        wait_bytes(part_recv.at[pl.ds(0, KV - 1)], part_rs)

    with jax.named_scope("combine"):
        tops, sums = [], []
        best = new_score
        for i in range(KV):
            stats = part_recv[i, :, LATENT:].astype(F32)
            top = stats[:, 0:1] + stats[:, 1:2] + stats[:, 2:3]
            tops.append(top)
            sums.append(stats[:, 3:4] + stats[:, 4:5] + stats[:, 5:6])
            best = jnp.maximum(best, top)
        new_weight = jnp.exp(new_score - best)
        weighted = rounded(new_weight) * new_key[:, :LATENT]
        weight_sum = new_weight
        for i in range(KV):
            share = jnp.exp(tops[i] - best)
            weight_sum = weight_sum + share * sums[i]
            weighted = weighted + share * part_recv[i, :, :LATENT].astype(F32)
        hl = (weighted / weight_sum).astype(BF16)
        ho_send[...] = dot(hl, wv_recv[0]).astype(BF16)
        slot = head * 16 + t * 2 + part
        ho_recv[slot] = ho_send[...]

    with jax.named_scope("send_ho"):
        for d in EVERYWHERE:
            remote(
                ho_send, ho_recv.at[slot], ss.at[4], ho_rs, at_plane(d[:2]), at_line(d[2:])
            ).start()

    with jax.named_scope("wait_ho"):
        load_gain[1].wait()
        wait_bytes(wo_all.at[pl.ds(0, TP - 1)], wo_rs)
        wait_bytes(ho_recv.at[pl.ds(0, KV * TP - 1)], ho_rs)

    with jax.named_scope("mix"):
        mixed = None
        for h in range(HEADS):
            block = jnp.concatenate(
                [ho_recv[h * 16 + j].astype(F32) for j in range(16)], axis=0
            ).astype(BF16)
            term = dot(block, wo_all[h])
            mixed = term if mixed is None else mixed + term
        squares = jnp.sum(mixed * mixed, axis=1, keepdims=True)
        diagonal = lax.broadcasted_iota(jnp.int32, (64, LANES), 0) == lane64
        sq_send[...] = jnp.sum(jnp.where(diagonal, squares, 0.0), axis=0, keepdims=True)
        sq_recv[k] = sq_send[...]

    with jax.named_scope("send_sq"):
        for d in PLANE:
            remote(sq_send, sq_recv.at[k], ss.at[5], sq_rs, at_plane(d), t).start()
        mixed = mixed * ogain[...]

    with jax.named_scope("drain"):
        wait_bytes(q_recv.at[pl.ds(0, KV - 1)], ss.at[0])

        @pl.when(jnp.logical_not(local_wv))
        def _():
            wait_bytes(wv_recv, ss.at[1])

        wait_bytes(wo_all.at[pl.ds(0, TP - 1)], ss.at[2])
        wait_bytes(part_recv.at[pl.ds(0, KV - 1)], ss.at[3])
        wait_bytes(ho_recv.at[pl.ds(0, KV * TP - 1)], ss.at[4])
        ql_all(pushed)
        for i in range(4):
            pushed(*row_args(i))

        def lat_done(i, carry):
            pushed(*lat_args(i))
            return carry

        lax.fori_loop(0, KV, lat_done, 0)

    with jax.named_scope("wait_sq"):
        wait_bytes(sq_recv.at[pl.ds(0, KV - 1)], sq_rs)

    with jax.named_scope("finish"):
        line = sq_recv[0]
        for i in range(1, KV):
            line = line + sq_recv[i]
        squares = jnp.sum(jnp.where(diagonal, line, 0.0), axis=1, keepdims=True)
        out[...] = (mixed * lax.rsqrt(squares / MODEL + EPSILON)).astype(out.dtype)
        wait_bytes(sq_recv.at[pl.ds(0, KV - 1)], ss.at[5])


def on_device(
    tokens,
    token_gain,
    w_query,
    w_down_kv,
    w_rope_key,
    latent_gain,
    w_key_up,
    w_value_up,
    w_out,
    out_gain,
    cache_latent,
    cache_rope,
    lengths,
):
    inverse = 1.0 / 10000.0 ** (np.arange(0, ROPE, 2, dtype=np.float32) / np.float32(ROPE))
    freq = jnp.asarray(np.tile(inverse.astype(np.float32), 4)[None, :])
    arrays = [
        freq,
        tokens,
        token_gain[None, :],
        w_query.T,
        w_down_kv,
        w_rope_key.T,
        w_key_up,
        cache_latent.reshape(SEQS * POS, LATENT),
        jnp.swapaxes(cache_rope, 1, 2).reshape(SEQS * ROPE, POS),
        latent_gain[None, :],
        w_value_up,
        w_out,
        out_gain[None, :],
    ]
    dma = lambda *n: pltpu.SemaphoreType.DMA(n)
    v = lambda *shape: pltpu.VMEM(shape, BF16)
    f = lambda *shape: pltpu.VMEM(shape, F32)
    return pl.pallas_call(
        kernel,
        out_shape=jax.ShapeDtypeStruct((64, LANES), BF16),
        in_specs=[pl.BlockSpec(memory_space=pltpu.SMEM)]
        + [pl.BlockSpec(memory_space=pl.ANY)] * len(arrays),
        out_specs=pl.BlockSpec(memory_space=pltpu.VMEM),
        scratch_shapes=[
            f(1, LANES),
            v(64, LANES),
            f(1, LANES),
            v(256, LANES),
            v(LANES, LATENT),
            v(LANES, LANES),
            v(1, LATENT, NOPE),
            v(SEQS * POS, LATENT),
            v(SEQS * ROPE, POS),
            f(1, LATENT),
            v(1, LATENT, NOPE),
            f(1, LANES),
            v(TP, LANES, LANES),
            v(NOPE, LATENT),
            v(SEQS * LATENT, POS),
            f(TP, SEQS, LANES),
            v(4, 16, 256),
            v(KV, 16, 256),
            f(SEQS, 1, FULL),
            f(KV, 1, FULL),
            f(1, FULL),
            f(ROWS, 1, FULL),
            v(2, SEQS, FULL),
            v(HEADS, SEQS, FULL),
            v(64, SEQS * LATENT),
            v(64, SEQS * ROPE),
            v(64, SEQS * POS),
            v(KV, ROWS, FULL),
            v(KV, ROWS, FULL),
            v(1, LATENT, NOPE),
            v(ROWS, LANES),
            v(KV * TP, ROWS, LANES),
            f(1, LANES),
            f(KV, 1, LANES),
            dma(14),
            dma(6),
            dma(),
            dma(KV),
            dma(ROWS),
            dma(HEADS),
            dma(),
            dma(),
            dma(),
            dma(),
            dma(),
            dma(8),
            dma(4),
            dma(KV),
        ],
        compiler_params=pltpu.CompilerParams(
            collective_id=0, has_side_effects=True, vmem_limit_bytes=56 * 1024 * 1024
        ),
        name="decode",
    )(lengths, *arrays)


def solution(mesh):
    placed = (
        P(None, "kv"),
        P("kv"),
        P("kv", "tp"),
        P("kv", None),
        P("kv", None),
        P(),
        P("tp", None, None),
        P("tp", None, None),
        P("tp", "kv"),
        P("kv"),
        P("tp", "kv", None),
        P("tp", "kv", None),
        P(),
    )
    return jax.shard_map(
        on_device,
        mesh=mesh,
        in_specs=placed,
        out_specs=P(None, "kv"),
        check_vma=False,
    )
```

time: 50.5 us -> 38.2 us (0.76)
  Pallas kernels: 45.6 us -> 36.6 us
  local copies, waits for them, and re-layouts: 2.99 us -> 1.32 us
  other arithmetic: 1.57 us -> 0 us
    pallas_call x1, Pallas kernels: 45.6 us -> 36.6 us  [on_device(): pl.pallas_call(kernel, out_shape=jax.ShapeDtypeStruct((64, LANES), BF16),...]
    unnamed x2 -> x1, local copies, waits for them, and re-layouts: 2.84 us -> 1.32 us
    concatenate x1 -> x0, other arithmetic: 0.71 us -> none  [on_device(): sin = jnp.concatenate([-sine, sine, blank], axis=1).reshape(tp, seqs, LANES)]
    convert_element_type x1 -> x0, other arithmetic: 0.66 us -> none  [on_device(): angles = lengths.astype(F32)[:, None] * inverse_freq[None, :]]
where the time goes in v1:
time: 38.2 us; the launch traced here: 37.9 us
  Pallas kernels  36.6 us (96%)
  local copies, waits for them, and re-layouts  1.32 us (3%)
    pallas_call x1, Pallas kernels, on_device(): pl.pallas_call(kernel, out_shape=jax.ShapeDtypeStruct((64, LANES), BF16),...  36.6 us
    unnamed x1, local copies, waits for them, and re-layouts  1.32 us

profile of v1, /device:TPU:1, one launch (start us, length us, event | category | flops | bytes accessed | tf_op | source)
XLA Modules:
  0.0 37.9 jit_solution(6555680766472514093)
XLA Ops:
  0.0 36.6 %decode.1 = bf16[64,128]{1,0:T(8,128)(2,1)} custom-call(s32[64]{0:T(128)} %lengths.1, f32[1,128]{1,0:T(1,128)} %constant.2.clone.freq_h, bf16[64,128]{1,0:T(8,128)(2,1)} %tok_h.1, f32[1,128]{1,0:T(1,128)} %bitcast.14, bf16[192,128]{1,0:T(8,128)(2,1)} %bitcast.11, bf16[128,512]{1,0:T(8,128)(2,1)} %wd_h.1, bf16[64,128]{1,0:T(8,128)(2,1)} %bitcast.12, ...), custom_call_target="tpu_custom_call" | custom-call | tf_op jit(solution)/shard_map/decode/pallas_call | solution.py:552
  36.6 1.3 %copy.16 = bf16[64,128]{1,0:T(8,128)(2,1)} copy(bf16[64,128]{1,0:T(8,128)(2,1)} %decode.1) | data formatting | bytes 32768

commit v2 on v1

--- a/solution.py
+++ b/solution.py
@@ -24,7 +24,6 @@
 ROPE = 64
 POS = 512
 FULL = LATENT + LANES
-ROWS = 4
 FACTOR = (NOPE + ROPE) ** (-0.5)
 MODEL = 2048
 
@@ -41,11 +40,11 @@
     [(a, b) for a in range(SIDE) for b in range(2) if (a, b) != (0, 0)],
     key=lambda d: -(2 * ring_distance(d[0]) + d[1]),
 )
-EVERYWHERE = sorted(
+NEAR = ((0, 0), (0, 1), (0, 3), (1, 0), (3, 0), (0, 2), (1, 1), (1, 3))
+SERVED = sorted(
     [
         (a, b, c, d)
-        for a in range(SIDE)
-        for b in range(SIDE)
+        for a, b in NEAR
         for c in range(SIDE)
         for d in range(2)
         if (a, b, c, d) != (0, 0, 0, 0)
@@ -147,6 +146,18 @@
     z, x = k // SIDE, k % SIDE
     y, core = t // 2, t % 2
 
+    def at_plane(d):
+        return ((z + d[0]) % SIDE) * SIDE + (x + d[1]) % SIDE
+
+    def at_line(d):
+        return ((y + d[0]) % SIDE) * 2 + (core + d[1]) % 2
+
+    barrier = pltpu.get_barrier_semaphore()
+    for d in PLANE:
+        pl.semaphore_signal(barrier, inc=1, device_id=(at_plane(d), t), device_id_type=MESH)
+    for d in LINE:
+        pl.semaphore_signal(barrier, inc=1, device_id=(k, at_line(d)), device_id_type=MESH)
+
     def load(i, a, b):
         copy = pltpu.make_async_copy(a, b, in_sem.at[i])
         copy.start()
@@ -167,21 +178,25 @@
     load_up = [load(7, wku_h, wku)]
     load_cl = [load(8, cl_h, cl)]
     load_cr = [load(9, cr_h, cr)]
-    load_wvu = load(10, wvu_h, wvu)
     load_wo = load(11, wo_h, wo_all.at[t])
     load_gain = [load(12, lgain_h, lgain), load(13, ogain_h, ogain)]
 
-    def at_plane(d):
-        return ((z + d[0]) % SIDE) * SIDE + (x + d[1]) % SIDE
-
-    def at_line(d):
-        return ((y + d[0]) % SIDE) * 2 + (core + d[1]) % 2
-
-    barrier = pltpu.get_barrier_semaphore()
-    for d in PLANE:
-        pl.semaphore_signal(barrier, inc=1, device_id=(at_plane(d), t), device_id_type=MESH)
-    for d in LINE:
-        pl.semaphore_signal(barrier, inc=1, device_id=(k, at_line(d)), device_id_type=MESH)
+    def head_of(d):
+        zz, xx = (z + d[0]) % SIDE, x + d[1]
+        m = (zz % 2) * SIDE + (xx + 2 * (zz // 2)) % SIDE
+        return ((y + m // 2) % SIDE) * 2 + (core + m % 2) % 2, m
+
+    head, shift = head_of((0, 0))
+    local_wv = shift == 0
+    wvu_load = pltpu.make_async_copy(wvu_h, wvu, in_sem.at[10])
+
+    @pl.when(local_wv)
+    def _():
+        pltpu.make_async_copy(wvu_h, wv_recv, wv_rs).start()
+
+    @pl.when(jnp.logical_not(local_wv))
+    def _():
+        wvu_load.start()
 
     def remote(src, dst, send, recv, kk, tt):
         return pltpu.make_async_remote_copy(
@@ -218,9 +233,12 @@
         for c in first:
             c.wait()
         scaled = (tok[...].astype(F32) * tgain[...]).astype(BF16)
-        query = dot_t(scaled, wq[...]).astype(BF16)
+        query = dot_t(scaled, wq[...])
         for p in range(4):
-            q_send[p] = query[16 * p : 16 * p + 16]
+            low, high = p * SEQS, (p + 4) * SEQS
+            q_send[p] = jnp.concatenate(
+                [query[low : low + SEQS], query[high : high + SEQS]], axis=0
+            ).astype(BF16)
         mine = (x + 2 * z) % 4
         q_recv[k] = q_send[mine]
         wide = scaled.astype(F32)
@@ -236,18 +254,13 @@
             server = ((x + d[1]) + 2 * (z + d[0])) % 4
             remote(q_send.at[server], q_recv.at[k], ss.at[0], q_rs, kk, t).start()
 
-    wv_to = ((y - z) % SIDE) * 2 + (core - x // 2) % 2
-    local_wv = jnp.logical_and(z == 0, x // 2 == 0)
+    wv_to = ((y + SIDE - shift // 2) % SIDE) * 2 + (core + shift % 2) % 2
     with jax.named_scope("send_wv"):
-        load_wvu.wait()
 
         @pl.when(jnp.logical_not(local_wv))
         def _():
+            wvu_load.wait()
             remote(wvu, wv_recv, ss.at[1], wv_rs, k, wv_to).start()
-
-        @pl.when(local_wv)
-        def _():
-            wv_recv[...] = wvu[...]
 
     with jax.named_scope("lat_partial"):
         for c in load_lat:
@@ -280,7 +293,7 @@
         row16 = lax.broadcasted_iota(jnp.int32, (16, LANES), 0)
         len16 = jnp.zeros((16, LANES), F32)
         for i in range(16):
-            len16 = jnp.where(row16 == i, lengths[mine * 16 + i].astype(F32), len16)
+            len16 = jnp.where(row16 == i, lengths[(mine + i // SEQS * 4) * SEQS + i % SEQS].astype(F32), len16)
         angle = len16 * freq[...]
         cos16 = jnp.cos(angle)
         sin16 = jnp.sin(angle) * sign
@@ -325,16 +338,11 @@
                     ql_ss.at[2 * j + g],
                     ql_rs.at[t],
                     at_plane(d),
-                    2 * mine + g,
+                    mine + 4 * g,
                 )
 
     with jax.named_scope("send_ql"):
         ql_all(push)
-
-    with jax.named_scope("send_wo"):
-        load_wo.wait()
-        for d in LINE:
-            remote(wo_all.at[t], wo_all.at[t], ss.at[2], wo_rs, k, at_line(d)).start()
 
     with jax.named_scope("new_row"):
         load_gain[0].wait()
@@ -349,13 +357,13 @@
         row_send[:, LATENT:] = rounded(rotated(fresh[:, LATENT:], cos1, sin1))
         row_args = lambda i: (
             row_send,
-            row_recv.at[seq % ROWS],
+            row_recv.at[seq],
             row_ss.at[i],
-            row_rs.at[seq % ROWS],
-            2 * (4 * (k % 2) + i) + seq // ROWS,
+            row_rs.at[seq],
+            k % 2 + 2 * i,
             t,
         )
-        for i in range(4):
+        for i in range(SEQS):
             push(*row_args(i))
 
     with jax.named_scope("masks"):
@@ -370,6 +378,11 @@
     with jax.named_scope("wait_ql"):
         for i in range(HEADS):
             wait_bytes(ql_recv.at[i], ql_rs.at[i])
+
+    with jax.named_scope("send_wo"):
+        load_wo.wait()
+        for d in LINE:
+            remote(wo_all.at[t], wo_all.at[t], ss.at[2], wo_rs, k, at_line(d)).start()
 
     with jax.named_scope("scores"):
         q = jnp.concatenate([ql_recv[i].astype(F32) for i in range(HEADS)], axis=0).astype(BF16)
@@ -400,34 +413,24 @@
                 value = value - bit
     with jax.named_scope("attend"):
         acc = dot(wm[...], cl[...])
-        for i in range(KV):
-            part_send[i, :, :LATENT] = acc[i * ROWS : (i + 1) * ROWS].astype(BF16)
-            part_send[i, :, LATENT:] = stats[i * ROWS : (i + 1) * ROWS].astype(BF16)
-
-    def head_of(zz, xx):
-        return ((y + zz) % SIDE) * 2 + (core + (xx % SIDE) // 2) % 2
-
-    head = head_of(z, x)
-    part = x % 2
+        for i in range(HEADS):
+            part_send[i, :, :LATENT] = acc[i * SEQS : (i + 1) * SEQS].astype(BF16)
+            part_send[i, :, LATENT:] = stats[i * SEQS : (i + 1) * SEQS].astype(BF16)
+
     with jax.named_scope("send_part"):
         for d in PLANE:
-            index = head_of(z + d[0], x + d[1]) * 2 + (x + d[1]) % 2
             remote(
-                part_send.at[index], part_recv.at[k], ss.at[3], part_rs, at_plane(d), t
+                part_send.at[head_of(d)[0]], part_recv.at[k], ss.at[3], part_rs, at_plane(d), t
             ).start()
-        part_recv[k] = part_send[head * 2 + part]
+        part_recv[k] = part_send[head]
 
     with jax.named_scope("new_score"):
-        for i in range(ROWS):
+        for i in range(SEQS):
             wait_bytes(row_recv.at[i], row_rs.at[i])
-        new_key = jnp.concatenate([row_recv[i] for i in range(ROWS)], axis=0)
+        new_key = jnp.concatenate([row_recv[i] for i in range(SEQS)], axis=0)
         own_query = ql_recv[head].astype(F32)
-        own_query = jnp.where(part == 0, own_query[:ROWS], own_query[ROWS:])
         new_score = jnp.sum(own_query * new_key, axis=1, keepdims=True) * FACTOR
-
-        @pl.when(jnp.logical_not(local_wv))
-        def _():
-            wait_bytes(wv_recv, wv_rs)
+        wait_bytes(wv_recv, wv_rs)
 
     with jax.named_scope("wait_part"):
         wait_bytes(part_recv.at[pl.ds(0, KV - 1)], part_rs)
@@ -450,11 +453,11 @@
             weighted = weighted + share * part_recv[i, :, :LATENT].astype(F32)
         hl = (weighted / weight_sum).astype(BF16)
         ho_send[...] = dot(hl, wv_recv[0]).astype(BF16)
-        slot = head * 16 + t * 2 + part
+        slot = head * TP + t
         ho_recv[slot] = ho_send[...]
 
     with jax.named_scope("send_ho"):
-        for d in EVERYWHERE:
+        for d in SERVED:
             remote(
                 ho_send, ho_recv.at[slot], ss.at[4], ho_rs, at_plane(d[:2]), at_line(d[2:])
             ).start()
@@ -462,13 +465,13 @@
     with jax.named_scope("wait_ho"):
         load_gain[1].wait()
         wait_bytes(wo_all.at[pl.ds(0, TP - 1)], wo_rs)
-        wait_bytes(ho_recv.at[pl.ds(0, KV * TP - 1)], ho_rs)
+        wait_bytes(ho_recv.at[pl.ds(0, HEADS * TP - 1)], ho_rs)
 
     with jax.named_scope("mix"):
         mixed = None
         for h in range(HEADS):
             block = jnp.concatenate(
-                [ho_recv[h * 16 + j].astype(F32) for j in range(16)], axis=0
+                [ho_recv[h * TP + j].astype(F32) for j in range(TP)], axis=0
             ).astype(BF16)
             term = dot(block, wo_all[h])
             mixed = term if mixed is None else mixed + term
@@ -491,9 +494,9 @@
 
         wait_bytes(wo_all.at[pl.ds(0, TP - 1)], ss.at[2])
         wait_bytes(part_recv.at[pl.ds(0, KV - 1)], ss.at[3])
-        wait_bytes(ho_recv.at[pl.ds(0, KV * TP - 1)], ss.at[4])
+        wait_bytes(ho_recv.at[pl.ds(0, HEADS * TP - 1)], ss.at[4])
         ql_all(pushed)
-        for i in range(4):
+        for i in range(SEQS):
             pushed(*row_args(i))
 
         def lat_done(i, carry):
@@ -551,7 +554,7 @@
     f = lambda *shape: pltpu.VMEM(shape, F32)
     return pl.pallas_call(
         kernel,
-        out_shape=jax.ShapeDtypeStruct((64, LANES), BF16),
+        out_shape=pltpu.VMEM((64, LANES), BF16),
         in_specs=[pl.BlockSpec(memory_space=pltpu.SMEM)]
         + [pl.BlockSpec(memory_space=pl.ANY)] * len(arrays),
         out_specs=pl.BlockSpec(memory_space=pltpu.VMEM),
@@ -577,24 +580,24 @@
             f(SEQS, 1, FULL),
             f(KV, 1, FULL),
             f(1, FULL),
-            f(ROWS, 1, FULL),
+            f(SEQS, 1, FULL),
             v(2, SEQS, FULL),
             v(HEADS, SEQS, FULL),
             v(64, SEQS * LATENT),
             v(64, SEQS * ROPE),
             v(64, SEQS * POS),
-            v(KV, ROWS, FULL),
-            v(KV, ROWS, FULL),
+            v(HEADS, SEQS, FULL),
+            v(KV, SEQS, FULL),
             v(1, LATENT, NOPE),
-            v(ROWS, LANES),
-            v(KV * TP, ROWS, LANES),
+            v(SEQS, LANES),
+            v(HEADS * TP, SEQS, LANES),
             f(1, LANES),
             f(KV, 1, LANES),
             dma(14),
             dma(6),
             dma(),
             dma(KV),
-            dma(ROWS),
+            dma(SEQS),
             dma(HEADS),
             dma(),
             dma(),
@@ -602,7 +605,7 @@
             dma(),
             dma(),
             dma(8),
-            dma(4),
+            dma(8),
             dma(KV),
         ],
         compiler_params=pltpu.CompilerParams(

time: 38.2 us -> 35.8 us (0.937)
  Pallas kernels: 36.6 us -> 34.8 us
  local copies, waits for them, and re-layouts: 1.32 us -> 0.61 us
    pallas_call x1, Pallas kernels: 36.6 us -> 34.8 us  [on_device(): pl.pallas_call(kernel, out_shape=pltpu.VMEM((64, LANES), BF16), in_specs=...]
    unnamed x1, local copies, waits for them, and re-layouts: 1.32 us -> 0.61 us
where the time goes in v2:
time: 35.8 us; the launch traced here: 35.4 us
  Pallas kernels  34.8 us (97%)
  local copies, waits for them, and re-layouts  0.61 us (2%)
    pallas_call x1, Pallas kernels, on_device(): pl.pallas_call(kernel, out_shape=pltpu.VMEM((64, LANES), BF16), in_specs=...  34.8 us

profile of v2, /device:TPU:1, one launch (start us, length us, event | category | flops | bytes accessed | tf_op | source)
XLA Modules:
  0.0 35.4 jit_solution(5722784119619136189)
XLA Ops:
  0.0 34.8 %decode.1 = bf16[64,128]{1,0:T(8,128)(2,1)S(1)} custom-call(s32[64]{0:T(128)} %lengths.1, f32[1,128]{1,0:T(1,128)} %constant.2.clone.freq_h, bf16[64,128]{1,0:T(8,128)(2,1)} %tok_h.1, f32[1,128]{1,0:T(1,128)} %bitcast.14, bf16[192,128]{1,0:T(8,128)(2,1)} %bitcast.11, bf16[128,512]{1,0:T(8,128)(2,1)} %wd_h.1, bf16[64,128]{1,0:T(8,128)(2,1)} %bitcast.12, ...), custom_call_target="tpu_custom_call" | custom-call | tf_op jit(solution)/shard_map/decode/pallas_call | solution.py:555
  34.8 0.6 %copy.16 = bf16[64,128]{1,0:T(8,128)(2,1)} copy(bf16[64,128]{1,0:T(8,128)(2,1)S(1)} %decode.1) | data formatting | bytes 32768
